TPU v7x, 32 devices: a whole 2x2x4 slice. The times are simulated.
32 devices in a mesh: fs: 16 (over z, y, core), tp: 2 (over x).
Axes of the slice: x: 2, y: 2, z: 4, core: 2. Of those that a mesh axis runs over, the one named last changes fastest.
Arguments:
- inputs: bfloat16 [16384, 3072], P('fs'), may hold values from -6 to 6
- query_cot: bfloat16 [16384, 768], P('fs', 'tp'), may hold values from -0.046875 to 0.046875
- value_cot: bfloat16 [16384, 1536], P('fs', 'tp'), may hold values from -0.046875 to 0.046875
- query_factor: bfloat16 [3072, 192], P('fs'), may hold values from -0.109375 to 0.109375
- value_factor: bfloat16 [3072, 192], P('fs'), may hold values from -0.109375 to 0.109375
- query_weight: float32 [3072, 768], P('fs', 'tp'), may hold values from -0.109375 to 0.109375
- value_weight: float32 [3072, 1536], P('fs', 'tp'), may hold values from -0.109375 to 0.109375
- query_first: float32 [192, 768], P('fs', 'tp'), may hold values from -1.6 to 1.6
- query_second: float32 [192, 768], P('fs', 'tp'), may hold values from 0.002 to 0.05
- value_first: float32 [192, 1536], P('fs', 'tp'), may hold values from -1.6 to 1.6
- value_second: float32 [192, 1536], P('fs', 'tp'), may hold values from 0.002 to 0.05
Outputs:
- step_q: float32 [3072, 768], P('fs', 'tp')
- step_v: float32 [3072, 1536], P('fs', 'tp')
- new_q: float32 [3072, 768], P('fs', 'tp')
- new_v: float32 [3072, 1536], P('fs', 'tp')
- first_q: float32 [192, 768], P('fs', 'tp')
- second_q: float32 [192, 768], P('fs', 'tp')
- first_v: float32 [192, 1536], P('fs', 'tp')
- second_v: float32 [192, 1536], P('fs', 'tp')
- copy_q: bfloat16 [3072, 768], P(None, 'tp')
- copy_v: bfloat16 [3072, 1536], P(None, 'tp')
All inputs are finite; a program needn't handle non-finite values.
Results may differ from a plain program's by a relative error of at most 0.0041.
Values may be sent and summed in bfloat16 or wider, within the bound.
A program may use at most 64 MiB of HBM per device.

v0:
```python
import jax
import jax.numpy as jnp
from jax import lax
from jax.sharding import PartitionSpec as P

first_decay = 0.9
second_decay = 0.99
small_eps = 1e-08
learn_rate = 0.01


def moments(old_first, old_second, gradient):
    first = first_decay * old_first + (1.0 - first_decay) * gradient
    second = second_decay * old_second + (1.0 - second_decay) * gradient * gradient
    unit = first / (jnp.sqrt(second) + small_eps)
    return (first, second, unit)


def on_device(
    inputs,
    query_cot,
    value_cot,
    query_factor,
    value_factor,
    query_weight,
    value_weight,
    query_first,
    query_second,
    value_first,
    value_second,
):
    rank_cols = query_factor.shape[1]
    q_cols = query_cot.shape[1]
    v_cols = value_cot.shape[1]
    own_rows = query_first.shape[0]
    entries = rank_cols * (q_cols + v_cols) * lax.axis_size("tp")
    full_qf, full_vf = (
        lax.all_gather(query_factor, "fs", axis=0, tiled=True),
        lax.all_gather(value_factor, "fs", axis=0, tiled=True),
    )
    sum_q = jnp.dot(inputs, full_qf, preferred_element_type=jnp.float32)
    sum_v = jnp.dot(inputs, full_vf, preferred_element_type=jnp.float32)
    proj_q = sum_q.astype(jnp.bfloat16)
    proj_v = sum_v.astype(jnp.bfloat16)
    term_q = lax.dot_general(
        proj_q, query_cot, (((0,), (0,)), ((), ())), preferred_element_type=jnp.float32
    )
    term_v = lax.dot_general(
        proj_v, value_cot, (((0,), (0,)), ((), ())), preferred_element_type=jnp.float32
    )
    full_sums = lax.psum(jnp.concatenate([term_q, term_v], axis=1), "fs")
    stacked = (
        lax.all_gather(query_first, "fs", axis=0, tiled=True),
        lax.all_gather(query_second, "fs", axis=0, tiled=True),
        lax.all_gather(value_first, "fs", axis=0, tiled=True),
        lax.all_gather(value_second, "fs", axis=0, tiled=True),
    )
    all_first_q, all_second_q, unit_q = moments(stacked[0], stacked[1], full_sums[:, :q_cols])
    all_first_v, all_second_v, unit_v = moments(stacked[2], stacked[3], full_sums[:, q_cols:])
    norm_total = lax.psum(jnp.sum(unit_q * unit_q) + jnp.sum(unit_v * unit_v), "tp")
    step_scale = lax.rsqrt(norm_total / entries + 1e-06)
    whole_q = (step_scale * unit_q).astype(jnp.bfloat16)
    whole_v = (step_scale * unit_v).astype(jnp.bfloat16)
    row_begin = lax.axis_index("fs") * own_rows
    first_q = lax.dynamic_slice_in_dim(all_first_q, row_begin, own_rows, 0)
    second_q = lax.dynamic_slice_in_dim(all_second_q, row_begin, own_rows, 0)
    first_v = lax.dynamic_slice_in_dim(all_first_v, row_begin, own_rows, 0)
    second_v = lax.dynamic_slice_in_dim(all_second_v, row_begin, own_rows, 0)
    step_q = jnp.dot(query_factor, whole_q, preferred_element_type=jnp.float32)
    step_v = jnp.dot(value_factor, whole_v, preferred_element_type=jnp.float32)
    new_q = query_weight - learn_rate * step_q
    new_v = value_weight - learn_rate * step_v
    copy_q, copy_v = (
        lax.all_gather(new_q.astype(jnp.bfloat16), "fs", axis=0, tiled=True),
        lax.all_gather(new_v.astype(jnp.bfloat16), "fs", axis=0, tiled=True),
    )
    return (step_q, step_v, new_q, new_v, first_q, second_q, first_v, second_v, copy_q, copy_v)


def solution(mesh):
    in_specs = (
        P("fs", None),
        P("fs", "tp"),
        P("fs", "tp"),
        P("fs", None),
        P("fs", None),
        P("fs", "tp"),
        P("fs", "tp"),
        P("fs", "tp"),
        P("fs", "tp"),
        P("fs", "tp"),
        P("fs", "tp"),
    )
    out_specs = (
        P("fs", "tp"),
        P("fs", "tp"),
        P("fs", "tp"),
        P("fs", "tp"),
        P("fs", "tp"),
        P("fs", "tp"),
        P("fs", "tp"),
        P("fs", "tp"),
        P(None, "tp"),
        P(None, "tp"),
    )
    return jax.shard_map(
        on_device, mesh=mesh, in_specs=in_specs, out_specs=out_specs, check_vma=False
    )
```

profile of v0, /device:TPU:0, one launch (start us, length us, event | category | flops | bytes accessed | tf_op | source)
XLA Modules:
  0.0 321.6 jit_solution(11538157095303594677)
XLA Ops:
  7.2 0.0 copy-start
  7.2 0.0 copy-start.8
  7.2 0.0 all-gather.11.cloned.1.call-start
  7.2 0.7 all-gather.11.cloned.1.call-update
  7.9 0.0 all-gather.9.cloned.1.call-start
  8.0 0.7 all-gather.9.cloned.1.call-update
  8.7 0.0 all-reduce.2.cloned.1.call-start
  8.7 24.6 %all-gather = f32[16,12,384]{2,1,0:T(8,128)S(1)} all-gather(f32[1,12,384]{2,1,0:T(8,128)} %bitcast.18), channel_id=1, replica_groups=mesh['fs'=16,'tp'=2] {'fs'}, dimensions={0}, use_global_device_ids=true | all-gather | bytes 313344 | tf_op jit(solution)/shard_map/all_gather | solution.py:53
  33.4 21.9 %all-gather.2 = f32[16,12,768]{2,1,0:T(8,128)S(1)} all-gather(f32[1,12,768]{2,1,0:T(8,128)} %bitcast.16), channel_id=1, replica_groups=mesh['fs'=16,'tp'=2] {'fs'}, dimensions={0}, use_global_device_ids=true | all-gather | bytes 626688 | tf_op jit(solution)/shard_map/all_gather | solution.py:55
  55.3 0.1 broadcast_multiply_fusion.1
  55.4 0.0 copy-done.8
  55.4 21.1 %all-gather.3 = f32[16,12,768]{2,1,0:T(8,128)S(1)} all-gather(f32[1,12,768]{2,1,0:T(8,128)S(1)} %bitcast.17), channel_id=1, replica_groups=mesh['fs'=16,'tp'=2] {'fs'}, dimensions={0}, use_global_device_ids=true | all-gather | bytes 626688 | tf_op jit(solution)/shard_map/all_gather | solution.py:56
  76.5 0.1 broadcast_multiply_fusion
  76.6 0.0 all-gather.11.cloned.1.call-done
  76.6 0.0 copy-done
  76.6 6.6 %fusion.1 = f32[192,768]{1,0:T(8,128)} fusion(bf16[1024,768]{1,0:T(8,128)(2,1)S(1)} %copy-done, bf16[1024,3072]{1,0:T(8,128)(2,1)} %param.11, bf16[3072,192]{1,0:T(8,128)(2,1)} %all-gather.11.cloned.1.call-done), kind=kOutput, calls=%fused_computation.5 | convolution fusion | flops 1510146048 | bytes 9633792 | tf_op jit(solution)/shard_map/dot_general | solution.py:48
  83.3 15.3 %all-gather.9.cloned.1.call-done = bf16[3072,192]{1,0:T(8,128)(2,1)} async-done(((bf16[192,192]{1,0:T(8,128)(2,1)}), bf16[3072,192]{1,0:T(8,128)(2,1)}) %all-gather.9.cloned.1.call-update) | async-done | bytes 1179664 | tf_op jit(solution)/shard_map/all_gather | solution.py:38
  98.5 6.5 %fusion = f32[192,384]{1,0:T(8,128)} fusion(bf16[1024,384]{1,0:T(8,128)(2,1)} %param.12, bf16[1024,3072]{1,0:T(8,128)(2,1)} %param.11, bf16[3072,192]{1,0:T(8,128)(2,1)} %all-gather.9.cloned.1.call-done), kind=kOutput, calls=%fused_computation.4 | convolution fusion | flops 1359151104 | bytes 8552448 | tf_op jit(solution)/shard_map/dot_general | solution.py:45
  105.0 2.1 pad_maximum_fusion
  107.2 0.0 all-reduce.2.cloned.1.call-update
  107.2 0.0 all-gather.13.cloned.1.call-start
  107.2 0.8 broadcast_multiply_fusion.3
  108.0 0.9 reshape.33
  108.9 0.0 copy-start.3
  108.9 0.0 copy-start.9
  108.9 0.9 reshape.35
  109.8 0.2 copy-done.3
  110.0 0.0 copy-start.2
  110.0 0.7 reshape.29
  110.7 0.0 copy-done.9
  110.7 20.7 %all-gather.1 = f32[16,12,384]{2,1,0:T(8,128)S(1)} all-gather(f32[1,12,384]{2,1,0:T(8,128)S(1)} %bitcast.19), channel_id=1, replica_groups=mesh['fs'=16,'tp'=2] {'fs'}, dimensions={0}, use_global_device_ids=true | all-gather | bytes 313344 | tf_op jit(solution)/shard_map/all_gather | solution.py:54
  131.4 0.7 reshape.31
  132.2 0.0 copy-start.7
  132.2 67.6 %all-reduce.2.cloned.1.call-done = f32[192,1152]{1,0:T(8,128)} async-done(((f32[192,1152]{1,0:T(8,128)}), f32[192,1152]{1,0:T(8,128)}) %all-reduce.2.cloned.1.call-update) | async-done | bytes 884752 | tf_op jit(solution)/shard_map/psum | solution.py:51
  199.7 0.0 copy-done.2
  199.7 0.0 copy-start.4
  199.7 0.0 copy-start.5
  199.7 2.2 multiply_reduce_fusion
  202.0 0.0 copy-done.4
  202.0 0.0 copy-done.5
  202.0 0.0 copy-start.6
  202.0 1.8 multiply_reduce_fusion.1
  205.1 5.4 %psum.15 = f32[]{:T(128)} all-reduce(f32[]{:T(128)S(6)} %add.48), channel_id=1, replica_groups=mesh['fs'=16,'tp'=2] {'tp'}, use_global_device_ids=true, to_apply=%region_3.0 | all-reduce | flops 1 | bytes 8 | tf_op jit(solution)/shard_map/psum | solution.py:60
  211.2 0.0 copy-done.7
  211.2 2.1 fusion.7
  213.3 0.0 all-gather.13.cloned.1.call-update
  213.3 0.0 all-gather.15.cloned.1.call-start
  213.4 0.0 copy-done.6
  213.4 2.6 fusion.6
  216.0 0.0 all-gather.15.cloned.1.call-update
  216.0 0.6 constant_dynamic-slice_fusion.2
  216.7 0.6 constant_dynamic-slice_fusion
  217.3 37.5 %all-gather.13.cloned.1.call-done = bf16[3072,384]{1,0:T(8,128)(2,1)} async-done(((bf16[192,384]{1,0:T(8,128)(2,1)}), bf16[3072,384]{1,0:T(8,128)(2,1)}) %all-gather.13.cloned.1.call-update) | async-done | bytes 2359312 | tf_op jit(solution)/shard_map/all_gather | solution.py:74
  254.8 54.6 %all-gather.15.cloned.1.call-done = bf16[3072,768]{1,0:T(8,128)(2,1)} async-done(((bf16[192,768]{1,0:T(8,128)(2,1)}), bf16[3072,768]{1,0:T(8,128)(2,1)}) %all-gather.15.cloned.1.call-update) | async-done | bytes 4718608 | tf_op jit(solution)/shard_map/all_gather | solution.py:75
  309.4 0.0 copy-start.1
  309.4 3.5 %copy.24 = bf16[3072,384]{1,0:T(8,128)(2,1)} copy(bf16[3072,384]{1,0:T(8,128)(2,1)} %all-gather.13.cloned.1.call-done) | data formatting | bytes 4718592
  312.8 0.0 copy-done.1
  312.8 2.2 copy.25
  (1 shorter events, 0.0 us)
Async XLA Ops:
  7.2 69.5 %copy-start = (bf16[1024,768]{1,0:T(8,128)(2,1)S(1)}, bf16[1024,768]{1,0:T(8,128)(2,1)}, u32[]{:S(2)}) copy-start(bf16[1024,768]{1,0:T(8,128)(2,1)} %param.13) | copy-start | bytes 4718596
  7.2 48.2 %copy-start.8 = (f32[12,768]{1,0:T(8,128)S(1)}, f32[12,768]{1,0:T(8,128)}, u32[]{:S(2)}) copy-start(f32[12,768]{1,0:T(8,128)} %param.21) | copy-start | bytes 110596
  7.2 69.4 %all-gather.11.cloned.1.call-start = ((), (), s32[]{:S(2)}) async-start(), calls=%async_computation.1 | async-start | bytes 1671168 | tf_op jit(solution)/shard_map/all_gather | solution.py:39
  7.9 90.6 %all-gather.9.cloned.1.call-start = ((), (), s32[]{:S(2)}) async-start(), calls=%async_computation | async-start | bytes 1671168 | tf_op jit(solution)/shard_map/all_gather | solution.py:38
  8.7 191.0 %all-reduce.2.cloned.1.call-start = ((), (), s32[]{:S(2)}) async-start(), calls=%async_computation.2 | async-start | bytes 1769472 | tf_op jit(solution)/shard_map/psum | solution.py:51
  107.2 147.6 %all-gather.13.cloned.1.call-start = ((), (), s32[]{:S(2)}) async-start(), calls=%async_computation.3 | async-start | bytes 2506752 | tf_op jit(solution)/shard_map/all_gather | solution.py:74
  108.9 1.1 copy-start.3
  108.9 1.8 copy-start.9
  110.0 89.8 %copy-start.2 = (f32[192,768]{1,0:T(8,128)S(1)}, f32[192,768]{1,0:T(8,128)}, u32[]{:S(2)}) copy-start(f32[192,768]{1,0:T(8,128)} %reshape.33) | copy-start | bytes 1769476
  132.2 79.0 %copy-start.7 = (bf16[192,192]{1,0:T(8,128)(2,1)S(1)}, bf16[192,192]{1,0:T(8,128)(2,1)}, u32[]{:S(2)}) copy-start(bf16[192,192]{1,0:T(8,128)(2,1)} %param.14) | copy-start | bytes 221188
  199.7 2.2 copy-start.4
  199.7 2.2 copy-start.5
  202.0 11.4 %copy-start.6 = (bf16[192,192]{1,0:T(8,128)(2,1)S(1)}, bf16[192,192]{1,0:T(8,128)(2,1)}, u32[]{:S(2)}) copy-start(bf16[192,192]{1,0:T(8,128)(2,1)} %param.15) | copy-start | bytes 221188
  213.3 96.0 %all-gather.15.cloned.1.call-start = ((), (), s32[]{:S(2)}) async-start(), calls=%async_computation.4 | async-start | bytes 5013504 | tf_op jit(solution)/shard_map/all_gather | solution.py:75
  309.4 3.5 %copy-start.1 = (bf16[3072,768]{1,0:T(8,128)(2,1)S(1)}, bf16[3072,768]{1,0:T(8,128)(2,1)}, u32[]{:S(2)}) copy-start(bf16[3072,768]{1,0:T(8,128)(2,1)} %all-gather.15.cloned.1.call-done) | copy-start | bytes 14155780
Sparse Core Ops, SparseCore 0:
  10.3 43.8 all-gather.10
  56.4 42.0 all-gather.8
  107.3 92.3 all-reduce.1
  213.5 41.3 all-gather.12
  257.5 51.8 all-gather.14
where the time goes:
time: 322 us
  waiting for transfers between devices  176 us (55%)
  blocking collectives  93.8 us (29%)
  matrix products  17.9 us (6%)
  between operations  15.9 us (5%)
  local copies, waits for them, and re-layouts  10.4 us (3%)
  other arithmetic  7.08 us (2%)
    psum x1, waiting for transfers between devices, on_device(): full_sums = lax.psum(jnp.concatenate([term_q, term_v], axis=1), 'fs')  67.6 us
    all_gather x1, waiting for transfers between devices, on_device(): lax.all_gather(new_v.astype(jnp.bfloat16), 'fs', axis=0, tiled=True)  54.6 us
    all_gather x1, waiting for transfers between devices, on_device(): lax.all_gather(new_q.astype(jnp.bfloat16), 'fs', axis=0, tiled=True)  37.5 us
    all_gather x1, blocking collectives, on_device(): lax.all_gather(query_first, 'fs', axis=0, tiled=True)  24.6 us
    all_gather x1, blocking collectives, on_device(): lax.all_gather(value_first, 'fs', axis=0, tiled=True)  21.9 us
    all_gather x1, blocking collectives, on_device(): lax.all_gather(value_second, 'fs', axis=0, tiled=True)  21.1 us
    all_gather x1, blocking collectives, on_device(): lax.all_gather(query_second, 'fs', axis=0, tiled=True)  20.7 us
    all_gather x1, waiting for transfers between devices, on_device(): lax.all_gather(query_factor, 'fs', axis=0, tiled=True)  15.3 us
  transfers between devices with their start and end apart: 5, of which 4 were waited for; matrix products, arithmetic and copies ran while one was open for 5% of the time, Pallas kernels for 0%

commit v1 on v0

--- a/solution.py
+++ b/solution.py
@@ -48,7 +48,7 @@
     term_v = lax.dot_general(
         proj_v, value_cot, (((0,), (0,)), ((), ())), preferred_element_type=jnp.float32
     )
-    full_sums = lax.psum(jnp.concatenate([term_q, term_v], axis=1), "fs")
+    full_sums = jnp.sum(lax.all_gather(jnp.concatenate([term_q, term_v], axis=1), "fs"), axis=0)
     stacked = (
         lax.all_gather(query_first, "fs", axis=0, tiled=True),
         lax.all_gather(query_second, "fs", axis=0, tiled=True),

time: 322 us -> 350 us (1.087)
  waiting for transfers between devices: 176 us -> 195 us
  other arithmetic: 7.08 us -> 11.4 us
  blocking collectives: 93.8 us -> 97.9 us
    psum x1 -> x0, waiting for transfers between devices: 67.6 us -> none  [on_device(): full_sums = lax.psum(jnp.concatenate([term_q, term_v], axis=1), 'fs')]
    all_gather x1, waiting for transfers between devices: 0.02 us -> 43.9 us  [on_device(): lax.all_gather(value_factor, 'fs', axis=0, tiled=True)]
    all_gather x0 -> x1, waiting for transfers between devices: none -> 25.8 us  [on_device(): lax.all_gather(jnp.concatenate([term_q, term_v], axis=1), 'fs')]
    all_gather x1, waiting for transfers between devices: 15.3 us -> 34.8 us  [on_device(): lax.all_gather(query_factor, 'fs', axis=0, tiled=True)]
    reduce_sum x0 -> x1, other arithmetic: none -> 5.76 us  [on_device(): jnp.sum(lax.all_gather(jnp.concatenate([term_q, term_v], axis=1), 'fs'),...]
  transfers between devices with their start and end apart: 5 -> 5, of which waited for: 4 -> 5; matrix products, arithmetic and copies ran while one was open for 5% -> 4% of each run, Pallas kernels for 0% -> 0%
where the time goes in v1:
time: 350 us; the launch traced here: 349 us
  waiting for transfers between devices  195 us (56%)
  blocking collectives  97.9 us (28%)
  matrix products  16.4 us (5%)
  between operations  15.9 us (5%)
  local copies, waits for them, and re-layouts  11.9 us (3%)
  other arithmetic  11.4 us (3%)
    all_gather x1, waiting for transfers between devices, on_device(): lax.all_gather(new_v.astype(jnp.bfloat16), 'fs', axis=0, tiled=True)  54 us
    all_gather x1, waiting for transfers between devices, on_device(): lax.all_gather(value_factor, 'fs', axis=0, tiled=True)  43.9 us
    all_gather x1, waiting for transfers between devices, on_device(): lax.all_gather(new_q.astype(jnp.bfloat16), 'fs', axis=0, tiled=True)  35.3 us
    all_gather x1, waiting for transfers between devices, on_device(): lax.all_gather(query_factor, 'fs', axis=0, tiled=True)  34.8 us
    all_gather x1, waiting for transfers between devices, on_device(): lax.all_gather(jnp.concatenate([term_q, term_v], axis=1), 'fs')  25.8 us
    all_gather x1, blocking collectives, on_device(): lax.all_gather(value_second, 'fs', axis=0, tiled=True)  24.2 us
    all_gather x1, blocking collectives, on_device(): lax.all_gather(value_first, 'fs', axis=0, tiled=True)  23.7 us
    all_gather x1, blocking collectives, on_device(): lax.all_gather(query_second, 'fs', axis=0, tiled=True)  22.7 us
  transfers between devices with their start and end apart: 5, of which 5 were waited for; matrix products, arithmetic and copies ran while one was open for 4% of the time, Pallas kernels for 0%

profile of v1, /device:TPU:0, one launch (start us, length us, event | category | flops | bytes accessed | tf_op | source)
XLA Modules:
  0.0 349.1 jit_solution(1508407775567226340)
XLA Ops:
  7.2 0.0 copy-start
  7.2 0.0 all-gather.13.cloned.1.call-start
  7.2 0.7 all-gather.13.cloned.1.call-update
  7.9 0.0 all-gather.11.cloned.1.call-start
  8.0 0.7 all-gather.11.cloned.1.call-update
  8.7 0.0 copy-start.10
  8.7 0.0 all-gather.19.cloned.1.call-start
  8.7 43.9 %all-gather.13.cloned.1.call-done = bf16[3072,192]{1,0:T(8,128)(2,1)} async-done(((bf16[192,192]{1,0:T(8,128)(2,1)}), bf16[3072,192]{1,0:T(8,128)(2,1)}) %all-gather.13.cloned.1.call-update) | async-done | bytes 1179664 | tf_op jit(solution)/shard_map/all_gather | solution.py:39
  52.6 0.0 copy-done
  52.6 5.8 %fusion.1 = f32[192,768]{1,0:T(8,128)S(1)} fusion(bf16[1024,768]{1,0:T(8,128)(2,1)S(1)} %copy-done, bf16[1024,3072]{1,0:T(8,128)(2,1)} %param.11, bf16[3072,192]{1,0:T(8,128)(2,1)} %all-gather.13.cloned.1.call-done), kind=kOutput, calls=%fused_computation.5 | convolution fusion | flops 1510146048 | bytes 9633792 | tf_op jit(solution)/shard_map/dot_general | solution.py:48
  58.4 34.8 %all-gather.11.cloned.1.call-done = bf16[3072,192]{1,0:T(8,128)(2,1)} async-done(((bf16[192,192]{1,0:T(8,128)(2,1)}), bf16[3072,192]{1,0:T(8,128)(2,1)}) %all-gather.11.cloned.1.call-update) | async-done | bytes 1179664 | tf_op jit(solution)/shard_map/all_gather | solution.py:38
  93.3 0.0 copy-done.10
  93.3 5.6 %fusion = f32[192,384]{1,0:T(8,128)S(1)} fusion(bf16[1024,384]{1,0:T(8,128)(2,1)S(1)} %copy-done.10, bf16[1024,3072]{1,0:T(8,128)(2,1)} %param.11, bf16[3072,192]{1,0:T(8,128)(2,1)} %all-gather.11.cloned.1.call-done), kind=kOutput, calls=%fused_computation.4 | convolution fusion | flops 1359151104 | bytes 8552448 | tf_op jit(solution)/shard_map/dot_general | solution.py:45
  98.9 0.0 copy-start.6
  98.9 1.0 pad_maximum_fusion
  99.9 0.0 copy-start.7
  99.9 0.0 all-gather.19.cloned.1.call-update
  99.9 0.0 all-gather.15.cloned.1.call-start
  100.0 0.0 copy-done.6
  100.0 23.7 %all-gather.3 = f32[16,12,768]{2,1,0:T(8,128)S(1)} all-gather(f32[1,12,768]{2,1,0:T(8,128)S(1)} %bitcast.18), channel_id=1, replica_groups=mesh['fs'=16,'tp'=2] {'fs'}, dimensions={0}, use_global_device_ids=true | all-gather | bytes 626688 | tf_op jit(solution)/shard_map/all_gather | solution.py:55
  123.7 0.1 broadcast_multiply_fusion.1
  123.8 0.0 copy-start.8
  123.8 0.9 reshape.34
  124.7 0.0 copy-done.7
  124.7 24.2 %all-gather.4 = f32[16,12,768]{2,1,0:T(8,128)S(1)} all-gather(f32[1,12,768]{2,1,0:T(8,128)S(1)} %bitcast.19), channel_id=1, replica_groups=mesh['fs'=16,'tp'=2] {'fs'}, dimensions={0}, use_global_device_ids=true | all-gather | bytes 626688 | tf_op jit(solution)/shard_map/all_gather | solution.py:56
  148.9 0.0 copy-start.9
  148.9 0.1 broadcast_multiply_fusion
  149.0 0.9 reshape.36
  149.9 0.0 copy-done.8
  149.9 21.8 %all-gather.1 = f32[16,12,384]{2,1,0:T(8,128)S(1)} all-gather(f32[1,12,384]{2,1,0:T(8,128)S(1)} %bitcast.20), channel_id=1, replica_groups=mesh['fs'=16,'tp'=2] {'fs'}, dimensions={0}, use_global_device_ids=true | all-gather | bytes 313344 | tf_op jit(solution)/shard_map/all_gather | solution.py:53
  171.7 0.7 reshape.30
  172.4 0.0 copy-done.9
  172.4 22.7 %all-gather.2 = f32[16,12,384]{2,1,0:T(8,128)S(1)} all-gather(f32[1,12,384]{2,1,0:T(8,128)S(1)} %bitcast.21), channel_id=1, replica_groups=mesh['fs'=16,'tp'=2] {'fs'}, dimensions={0}, use_global_device_ids=true | all-gather | bytes 313344 | tf_op jit(solution)/shard_map/all_gather | solution.py:54
  195.2 0.7 reshape.32
  196.0 25.8 %all-gather.19.cloned.1.call-done = f32[3072,1152]{1,0:T(8,128)} async-done(((f32[192,1152]{1,0:T(8,128)}), f32[3072,1152]{1,0:T(8,128)}) %all-gather.19.cloned.1.call-update) | async-done | bytes 14155792 | tf_op jit(solution)/shard_map/all_gather | solution.py:51
  221.8 5.8 %reduce_sum.27 = f32[192,1152]{1,0:T(8,128)S(1)} reduce(f32[16,192,1152]{2,1,0:T(8,128)} %bitcast.17, f32[]{:T(128)} %constant.14.clone.1), dimensions={0}, to_apply=%region_0.0 | reduce | flops 3317760 | bytes 15040516 | tf_op jit(solution)/shard_map/reduce_sum | solution.py:51
  227.5 0.0 copy-start.2
  227.6 0.0 copy-start.3
  227.6 0.0 copy-start.5
  227.6 3.0 multiply_reduce_fusion
  230.6 0.0 copy-done.2
  230.6 0.0 copy-done.3
  230.6 0.0 copy-start.4
  230.6 1.5 multiply_reduce_fusion.1
  233.4 5.4 %psum.7 = f32[]{:T(128)} all-reduce(f32[]{:T(128)S(6)} %add.46), channel_id=1, replica_groups=mesh['fs'=16,'tp'=2] {'tp'}, use_global_device_ids=true, to_apply=%region_3.0 | all-reduce | flops 1 | bytes 8 | tf_op jit(solution)/shard_map/psum | solution.py:60
  239.5 0.0 copy-done.5
  239.5 2.2 fusion.7
  241.7 0.0 all-gather.15.cloned.1.call-update
  241.7 0.0 all-gather.17.cloned.1.call-start
  241.8 0.0 copy-done.4
  241.8 2.8 fusion.6
  244.6 0.0 all-gather.17.cloned.1.call-update
  244.6 1.4 constant_dynamic-slice_fusion.2
  246.0 1.5 constant_dynamic-slice_fusion
  247.5 35.3 %all-gather.15.cloned.1.call-done = bf16[3072,384]{1,0:T(8,128)(2,1)} async-done(((bf16[192,384]{1,0:T(8,128)(2,1)}), bf16[3072,384]{1,0:T(8,128)(2,1)}) %all-gather.15.cloned.1.call-update) | async-done | bytes 2359312 | tf_op jit(solution)/shard_map/all_gather | solution.py:74
  282.9 54.0 %all-gather.17.cloned.1.call-done = bf16[3072,768]{1,0:T(8,128)(2,1)} async-done(((bf16[192,768]{1,0:T(8,128)(2,1)}), bf16[3072,768]{1,0:T(8,128)(2,1)}) %all-gather.17.cloned.1.call-update) | async-done | bytes 4718608 | tf_op jit(solution)/shard_map/all_gather | solution.py:75
  336.9 0.0 copy-start.1
  336.9 3.5 copy.23
  340.3 0.0 copy-done.1
  340.3 2.2 copy.24
  (2 shorter events, 0.1 us)
Async XLA Ops:
  7.2 45.5 %copy-start = (bf16[1024,768]{1,0:T(8,128)(2,1)S(1)}, bf16[1024,768]{1,0:T(8,128)(2,1)}, u32[]{:S(2)}) copy-start(bf16[1024,768]{1,0:T(8,128)(2,1)} %param.13) | copy-start | bytes 4718596
  7.2 45.4 %all-gather.13.cloned.1.call-start = ((), (), s32[]{:S(2)}) async-start(), calls=%async_computation.1 | async-start | bytes 1671168 | tf_op jit(solution)/shard_map/all_gather | solution.py:39
  7.9 85.3 %all-gather.11.cloned.1.call-start = ((), (), s32[]{:S(2)}) async-start(), calls=%async_computation | async-start | bytes 1671168 | tf_op jit(solution)/shard_map/all_gather | solution.py:38
  8.7 84.6 %copy-start.10 = (bf16[1024,384]{1,0:T(8,128)(2,1)S(1)}, bf16[1024,384]{1,0:T(8,128)(2,1)}, u32[]{:S(2)}) copy-start(bf16[1024,384]{1,0:T(8,128)(2,1)} %param.12) | copy-start | bytes 2359300
  8.7 213.1 %all-gather.19.cloned.1.call-start = ((), (), s32[]{:S(2)}) async-start(), calls=%async_computation.4 | async-start | bytes 15040512 | tf_op jit(solution)/shard_map/all_gather | solution.py:51
  98.9 1.1 copy-start.6
  99.9 24.8 %copy-start.7 = (f32[12,768]{1,0:T(8,128)S(1)}, f32[12,768]{1,0:T(8,128)}, u32[]{:S(2)}) copy-start(f32[12,768]{1,0:T(8,128)} %param.21) | copy-start | bytes 110596
  99.9 183.0 %all-gather.15.cloned.1.call-start = ((), (), s32[]{:S(2)}) async-start(), calls=%async_computation.2 | async-start | bytes 2506752 | tf_op jit(solution)/shard_map/all_gather | solution.py:74
  123.8 26.1 %copy-start.8 = (f32[12,384]{1,0:T(8,128)S(1)}, f32[12,384]{1,0:T(8,128)}, u32[]{:S(2)}) copy-start(f32[12,384]{1,0:T(8,128)} %param.18) | copy-start | bytes 55300
  148.9 23.5 %copy-start.9 = (f32[12,384]{1,0:T(8,128)S(1)}, f32[12,384]{1,0:T(8,128)}, u32[]{:S(2)}) copy-start(f32[12,384]{1,0:T(8,128)} %param.19) | copy-start | bytes 55300
  227.5 3.1 copy-start.2
  227.6 3.1 copy-start.3
  227.6 11.9 %copy-start.5 = (bf16[192,192]{1,0:T(8,128)(2,1)S(1)}, bf16[192,192]{1,0:T(8,128)(2,1)}, u32[]{:S(2)}) copy-start(bf16[192,192]{1,0:T(8,128)(2,1)} %param.14) | copy-start | bytes 221188
  230.6 11.2 %copy-start.4 = (bf16[192,192]{1,0:T(8,128)(2,1)S(1)}, bf16[192,192]{1,0:T(8,128)(2,1)}, u32[]{:S(2)}) copy-start(bf16[192,192]{1,0:T(8,128)(2,1)} %param.15) | copy-start | bytes 221188
  241.7 95.1 %all-gather.17.cloned.1.call-start = ((), (), s32[]{:S(2)}) async-start(), calls=%async_computation.3 | async-start | bytes 5013504 | tf_op jit(solution)/shard_map/all_gather | solution.py:75
  336.9 3.5 copy-start.1
Sparse Core Ops, SparseCore 0:
  10.3 42.3 all-gather.12
  54.9 38.2 all-gather.10
  100.0 121.6 all-gather.18
  241.9 40.9 all-gather.14
  285.0 51.8 all-gather.16
